TPU v7x, 256 devices: a 4x2x16 block of a 4x16x16 slice. The times are simulated.
256 devices in a mesh: grp: 2 (over y), sp: 16 (over z), tp: 8 (over x, core).
Axes of the slice: x: 4, y: 2, z: 16, core: 2. Of those that a mesh axis runs over, the one named last changes fastest.
The devices are a block of a 4x16x16 slice.
Arguments:
- queries: bfloat16 [24576, 1024], P(('grp', 'sp'), 'tp'), parts along dimension 0, may hold values from -8 to 8
- keys: bfloat16 [24576, 256], P(('grp', 'sp')), parts along dimension 0, may hold values from -8 to 8
- values: bfloat16 [24576, 256], P(('grp', 'sp')), parts along dimension 0, may hold values from -6 to 6
- query_gain: float32 [128], replicated, may hold values from 0.2 to 6
- key_gain: float32 [128], replicated, may hold values from 0.2 to 6
- residual: bfloat16 [24576, 2048], P(('grp', 'sp', 'tp')), parts along dimension 0, may hold values from -6 to 6
- out_weight: bfloat16 [1024, 2048], P('tp'), may hold values from -0.1875 to 0.1875
- mix_gain: float32 [2048], replicated, may hold values from 0.1 to 1.9
- ffn_gain: float32 [2048], replicated, may hold values from 0.1 to 1.9
- gate_in: bfloat16 [2048, 5632], P('sp', 'tp'), may hold values from -0.125 to 0.125
- value_in: bfloat16 [2048, 5632], P('sp', 'tp'), may hold values from -0.125 to 0.125
- conv_gate: float32 [3, 5632], P(None, 'tp'), may hold values from -3 to 3
- conv_value: float32 [3, 5632], P(None, 'tp'), may hold values from -3 to 3
- down_t: bfloat16 [2048, 5632], P('sp', 'tp'), may hold values from -0.078125 to 0.078125
Outputs:
- layer_out: bfloat16 [24576, 2048], P(('grp', 'sp', 'tp')), parts along dimension 0
There are 2 independent parts, one for each index of `grp`. A program takes and returns all parts, laid end to end along the dimension named above; an argument that names none is the same for every part. Nothing has to cross between parts.
All inputs are finite; a program needn't handle non-finite values.
Results may differ from a plain program's by a relative error of at most 0.02.
The roundings to bfloat16 on the way count: a program that leaves them out, or rounds other values in their place, can miss the bound.
Values may be sent and summed in bfloat16 or wider, within the bound.
A program may use at most 128 MiB of HBM per device.

v0:
```python
import jax
import jax.numpy as jnp
from jax import lax
from jax.sharding import PartitionSpec as P

HEADS = 8
KVH = 2
GRID_W = 64
EPSILON = 1e-06
THETA = 10000.0


def sent_together(arrays, axis, dim, along):
    both = jnp.concatenate(arrays, axis=along)
    whole, at, gathered = (lax.all_gather(both, axis, axis=dim, tiled=True), 0, [])
    for a in arrays:
        gathered.append(lax.slice_in_dim(whole, at, at + a.shape[along], axis=along))
        at += a.shape[along]
    return tuple(gathered)


def cut_along(array, dim, size):
    before, after = (array.shape[:dim], array.shape[dim + 1 :])
    return jnp.moveaxis(array.reshape(*before, size, -1, *after), dim, 0)


def summed_on_arrival(array, axis, dim):
    tiles = cut_along(array, dim, lax.axis_size(axis))
    arrived = lax.all_to_all(tiles, axis, split_axis=0, concat_axis=0, tiled=True)
    return arrived.astype(jnp.float32).sum(axis=0)


def with_halo(block, sides, width):
    for axis, dim in sides:
        count = lax.axis_size(axis)
        forward = [(i, i + 1) for i in range(count - 1)]
        backward = [(target, source) for source, target in forward]
        low = lax.ppermute(
            lax.slice_in_dim(block, block.shape[dim] - width, None, axis=dim), axis, forward
        )
        high = lax.ppermute(lax.slice_in_dim(block, 0, width, axis=dim), axis, backward)
        block = jnp.concatenate([low, block, high], axis=dim)
    return block


def rotary_tables(positions, seq_total, head_dim):
    quarter = head_dim // 4
    inverse = THETA ** (-(2.0 * jnp.arange(quarter, dtype=jnp.float32)) / (head_dim // 2))
    grid_row = (positions // GRID_W - seq_total // GRID_W // 2).astype(jnp.float32)
    grid_col = (positions % GRID_W - GRID_W // 2).astype(jnp.float32)
    row_angle = grid_row[:, None] * inverse[None, :]
    col_angle = grid_col[:, None] * inverse[None, :]
    angle = jnp.concatenate([row_angle, row_angle, col_angle, col_angle], axis=-1)
    return (jnp.cos(angle), jnp.sin(angle))


def rotate_quarters(vector):
    first, second, third, fourth = jnp.split(vector, 4, axis=-1)
    return jnp.concatenate([-second, first, -fourth, third], axis=-1)


def prepare_heads(raw, gain, cos_table, sin_table, factor):
    floats = raw.astype(jnp.float32)
    normed = floats * lax.rsqrt(jnp.mean(floats * floats, axis=-1, keepdims=True) + EPSILON) * gain
    turned = normed * cos_table + rotate_quarters(normed) * sin_table
    return (turned * factor).astype(jnp.bfloat16)


def rms_rows(stream, gain):
    floats = stream.astype(jnp.float32)
    return floats * lax.rsqrt(jnp.mean(floats * floats, axis=-1, keepdims=True) + EPSILON) * gain


def body(
    queries,
    keys,
    values,
    query_gain,
    key_gain,
    residual,
    out_weight,
    mix_gain,
    ffn_gain,
    gate_in,
    value_in,
    conv_gate,
    conv_value,
    down_t,
):
    gate_rows, value_rows, down_rows = sent_together((gate_in, value_in, down_t), "sp", 0, 1)
    tok_rows = queries.shape[0]
    head_dim = query_gain.shape[0]
    local_heads = queries.shape[1] // head_dim
    seq_total = tok_rows * lax.axis_size("sp")
    kv_head = lax.axis_index("tp") * local_heads // (HEADS // KVH)
    positions = lax.axis_index("sp") * tok_rows + jnp.arange(tok_rows, dtype=jnp.int32)
    cos_table, sin_table = rotary_tables(positions, seq_total, head_dim)
    key_own = lax.dynamic_slice_in_dim(keys, kv_head * head_dim, head_dim, 1)
    value_own = lax.dynamic_slice_in_dim(values, kv_head * head_dim, head_dim, 1)
    key_rot = prepare_heads(key_own, key_gain, cos_table, sin_table, 1.0)
    query_rot = prepare_heads(
        queries.reshape(tok_rows, local_heads, head_dim),
        query_gain,
        cos_table[:, None, :],
        sin_table[:, None, :],
        head_dim ** (-0.5),
    )
    query_rows = jnp.transpose(query_rot, (1, 0, 2)).reshape(local_heads * tok_rows, head_dim)
    query_count = local_heads * tok_rows
    running = jnp.full((query_count, 1), -1e30, jnp.float32)
    key_piece, value_piece = sent_together((key_rot, value_own), "sp", 0, 1)
    scores = lax.dot_general(
        query_rows, key_piece, (((1,), (1,)), ((), ())), preferred_element_type=jnp.float32
    )
    newest = jnp.maximum(running, jnp.max(scores, axis=1, keepdims=True))
    weights = jnp.exp(scores - newest)
    denom = jnp.sum(weights, axis=1, keepdims=True)
    summed = jnp.dot(weights.astype(jnp.bfloat16), value_piece, preferred_element_type=jnp.float32)
    running, denom, summed = (newest, denom, summed)
    attended = (summed / denom).astype(jnp.bfloat16).reshape(local_heads, tok_rows, head_dim)
    attended = jnp.transpose(attended, (1, 0, 2)).reshape(tok_rows, local_heads * head_dim)
    block_rows = attended
    mix = summed_on_arrival(
        jnp.dot(block_rows, out_weight, preferred_element_type=jnp.float32).astype(jnp.bfloat16),
        "tp",
        0,
    )
    stream = (residual.astype(jnp.float32) + rms_rows(mix, mix_gain)).astype(jnp.bfloat16)
    normed = rms_rows(stream, ffn_gain).astype(jnp.bfloat16)
    paired = jnp.concatenate([gate_rows, value_rows], axis=1)
    upward = jnp.dot(
        lax.all_gather(normed, "tp", axis=0, tiled=True), paired, preferred_element_type=jnp.float32
    ).astype(jnp.bfloat16)
    padded = with_halo(upward, (("sp", 0),), 1).astype(jnp.float32)
    taps = jnp.concatenate([conv_gate, conv_value], axis=1)
    mixed = taps[0] * padded[:-2] + taps[1] * padded[1:-1] + taps[2] * padded[2:]
    unit_cols = conv_gate.shape[1]
    hidden = (jax.nn.gelu(mixed[:, :unit_cols], approximate=True) * mixed[:, unit_cols:]).astype(
        jnp.bfloat16
    )
    block_rows = hidden
    ffn_out = summed_on_arrival(
        lax.dot_general(
            block_rows, down_rows, (((1,), (1,)), ((), ())), preferred_element_type=jnp.float32
        ).astype(jnp.bfloat16),
        "tp",
        0,
    )
    return (stream.astype(jnp.float32) + ffn_out).astype(jnp.bfloat16)


def solution(mesh):
    return jax.shard_map(
        body,
        mesh=mesh,
        in_specs=(
            P(("grp", "sp"), "tp"),
            P(("grp", "sp"), None),
            P(("grp", "sp"), None),
            P(),
            P(),
            P(("grp", "sp", "tp"), None),
            P("tp", None),
            P(),
            P(),
            P("sp", "tp"),
            P("sp", "tp"),
            P(None, "tp"),
            P(None, "tp"),
            P("sp", "tp"),
        ),
        out_specs=P(("grp", "sp", "tp"), None),
        check_vma=False,
    )
```

profile of v0, /device:TPU:33, one launch (start us, length us, event | category | flops | bytes accessed | tf_op | source)
XLA Modules:
  0.0 345.3 jit_solution(11012669087130800998)
XLA Ops:
  6.6 1.2 fusion.55
  7.8 1.1 fusion.56
  8.9 0.4 slice_negate_fusion.1
  9.3 0.9 constant_dynamic-slice_fusion
  10.3 0.3 broadcast_multiply_fusion.1
  10.6 2.0 fusion.60
  12.6 0.8 pad_maximum_fusion.2
  13.5 1.9 pad_maximum_fusion
  15.6 0.2 fusion.48
  15.8 0.2 fusion.50
  16.0 0.4 fusion.58
  16.3 93.2 %all-gather.4.cloned.1.call-done = bf16[12288,256]{1,0:T(8,128)(2,1)} async-done(((bf16[768,256]{1,0:T(8,128)(2,1)}), bf16[12288,256]{1,0:T(8,128)(2,1)}) %all-gather.4.cloned.1.call-update) | async-done | bytes 6291472 | tf_op jit(solution)/shard_map/all_gather | solution.py:15
  109.5 16.3 %fusion.87 = (f32[768]{0:T(1024)S(1)}, f32[768,12288]{1,0:T(8,128)}) fusion(bf16[12288,256]{1,0:T(8,128)(2,1)} %all-gather.4.cloned.1.call-done, bf16[768,128]{1,0:T(8,128)(2,1)S(1)} %copy-done.2, f32[768,32]{1,0:T(8,128)S(1)} %get-tuple-element.13, f32[768,32]{1,0:T(8,128)S(1)} %get-tuple-element.14, f32[768,32]{1,0:T(8,128)S(1)} %get-tuple-element.15, ...), kind=kOutput, calls=%fused_computation.117 | convolution fusion | flops 2426731776 | bytes 41687552 | tf_op jit(solution)/shard_map/dot_general | solution.py:112
  125.9 15.4 %fusion = f32[768]{0:T(1024)S(1)} fusion(f32[768,12288]{1,0:T(8,128)} %get-tuple-element.23, f32[768]{0:T(1024)S(1)} %broadcast_maximum_fusion), kind=kLoop, calls=%fused_computation.1 | loop fusion | flops 18873600 | bytes 37754880 | tf_op jit(solution)/shard_map/reduce_sum | solution.py:117
  141.2 18.7 %convolution_convert_fusion.1 = bf16[768,2048]{1,0:T(8,128)(2,1)} fusion(bf16[128,2048]{1,0:T(8,128)(2,1)S(1)} %copy-done, bf16[12288,256]{1,0:T(8,128)(2,1)} %all-gather.4.cloned.1.call-done, f32[768,12288]{1,0:T(8,128)} %get-tuple-element.23, f32[768]{0:T(1024)S(1)} %broadcast_maximum_fusion, f32[768]{0:T(1024)S(1)} %fusion), kind=kOutput, calls=%fused_computation.16 | convolution fusion | flops 2839216128 | bytes 44570624 | tf_op jit(solution)/shard_map/dot_general | solution.py:124
  159.9 45.7 %all_to_all.10 = bf16[8,96,2048]{2,1,0:T(8,128)(2,1)S(1)} all-to-all(bf16[8,96,2048]{2,1,0:T(8,128)(2,1)} %bitcast.14), channel_id=1, replica_groups=mesh['grp'=2,'sp'=16,'tp'=8] {'tp'}, dimensions={0} | all-to-all | bytes 6291456 | tf_op jit(solution)/shard_map/all_to_all | solution.py:29
  205.6 0.6 convert_reduce_fusion.1
  206.2 0.1 multiply_reduce_fusion
  206.3 0.3 fusion.44
  206.7 0.9 fusion.46
  207.7 22.5 %all-gather.8.cloned.1.call-done = bf16[2048,2112]{0,1:T(8,128)(2,1)} async-done(((bf16[128,2112]{0,1:T(8,128)(2,1)}), bf16[2048,2112]{0,1:T(8,128)(2,1)}) %all-gather.8.cloned.1.call-update) | async-done | bytes 8650768 | tf_op jit(solution)/shard_map/all_gather | solution.py:15
  230.2 42.3 %all-gather.6.cloned.1.call-done = bf16[768,2048]{1,0:T(8,128)(2,1)} async-done(((bf16[96,2048]{1,0:T(8,128)(2,1)}), bf16[768,2048]{1,0:T(8,128)(2,1)}) %all-gather.6.cloned.1.call-update) | async-done | bytes 3145744 | tf_op jit(solution)/shard_map/all_gather | solution.py:132
  272.5 8.4 %fusion.9 = bf16[768,1408]{1,0:T(8,128)(2,1)S(1)} fusion(bf16[768,2048]{1,0:T(8,128)(2,1)} %all-gather.6.cloned.1.call-done, bf16[2048,2112]{0,1:T(8,128)(2,1)} %all-gather.8.cloned.1.call-done), kind=kOutput, calls=%fused_computation.17 | convolution fusion | flops 4430266368 | bytes 11075584 | tf_op jit(solution)/shard_map/dot_general | solution.py:131
  280.9 3.2 collective-permute-start
  284.1 1.3 collective-permute-start.1
  285.6 2.9 collective-permute-done.1
  288.5 0.4 maximum_convert_fusion
  288.9 1.3 fusion.7
  290.2 5.1 %convolution_convert_fusion = bf16[768,2048]{1,0:T(8,128)(2,1)S(1)} fusion(bf16[2048,2112]{0,1:T(8,128)(2,1)} %all-gather.8.cloned.1.call-done, f32[768,1408]{1,0:T(8,128)S(1)} %fusion.7), kind=kOutput, calls=%fused_computation.15 | convolution fusion | flops 2221572096 | bytes 10747904 | tf_op jit(solution)/shard_map/dot_general | solution.py:143
  295.3 42.0 %all_to_all.11 = bf16[8,96,2048]{2,1,0:T(8,128)(2,1)S(1)} all-to-all(bf16[8,96,2048]{2,1,0:T(8,128)(2,1)S(1)} %bitcast.15), channel_id=1, replica_groups=mesh['grp'=2,'sp'=16,'tp'=8] {'tp'}, dimensions={0} | all-to-all | bytes 6291456 | tf_op jit(solution)/shard_map/all_to_all | solution.py:29
  337.3 0.6 convert_reduce_fusion
  337.9 0.8 fusion.47
  (38 shorter events, 0.5 us)
Async XLA Ops:
  6.5 134.7 %copy-start = (bf16[128,2048]{1,0:T(8,128)(2,1)S(1)}, bf16[128,2048]{1,0:T(8,128)(2,1)}, u32[]{:S(2)}) copy-start(bf16[128,2048]{1,0:T(8,128)(2,1)} %param.20) | copy-start | bytes 1572868
  6.6 4.0 %copy-start.3 = (bf16[768,256]{1,0:T(8,128)(2,1)S(1)}, bf16[768,256]{1,0:T(8,128)(2,1)}, u32[]{:S(2)}) copy-start(bf16[768,256]{1,0:T(8,128)(2,1)} %param.15) | copy-start | bytes 1179652
  6.6 4.0 %copy-start.10 = (f32[128]{0:T(128)S(1)}, f32[128]{0:T(128)}, u32[]{:S(2)}) copy-start(f32[128]{0:T(128)} %param.18) | copy-start | bytes 1540
  6.6 103.0 %all-gather.4.cloned.1.call-start = ((), (), s32[]{:S(2)}) async-start(), calls=%async_computation.2 | async-start | bytes 6684672 | tf_op jit(solution)/shard_map/all_gather | solution.py:15
  8.9 6.6 %copy-start.2 = (bf16[768,128]{1,0:T(8,128)(2,1)S(1)}, bf16[768,128]{1,0:T(8,128)(2,1)}, u32[]{:S(2)}) copy-start(bf16[768,128]{1,0:T(8,128)(2,1)} %param.14) | copy-start | bytes 589828
  8.9 6.8 %copy-start.9 = (f32[128]{0:T(128)S(1)}, f32[128]{0:T(128)}, u32[]{:S(2)}) copy-start(f32[128]{0:T(128)} %param.17) | copy-start | bytes 1540
  13.4 216.8 %all-gather.8.cloned.1.call-start = ((), (), s32[]{:S(2)}) async-start(), calls=%async_computation.4 | async-start | bytes 9191424 | tf_op jit(solution)/shard_map/all_gather | solution.py:15
  15.5 257.0 %all-gather.6.cloned.1.call-start = ((), (), s32[]{:S(2)}) async-start(), calls=%async_computation.3 | async-start | bytes 3538944 | tf_op jit(solution)/shard_map/all_gather | solution.py:132
  159.9 46.4 %copy-start.4 = (bf16[96,2048]{1,0:T(8,128)(2,1)S(1)}, bf16[96,2048]{1,0:T(8,128)(2,1)}, u32[]{:S(2)}) copy-start(bf16[96,2048]{1,0:T(8,128)(2,1)} %param.19) | copy-start | bytes 1179652
  159.9 46.4 %copy-start.7 = (f32[2048]{0:T(1024)S(1)}, f32[2048]{0:T(1024)}, u32[]{:S(2)}) copy-start(f32[2048]{0:T(1024)} %param.21) | copy-start | bytes 24580
  205.6 1.1 copy-start.8
  207.7 77.8 %copy-start.5 = (f32[3,704]{1,0:T(4,128)S(1)}, f32[3,704]{1,0:T(4,128)}, u32[]{:S(2)}) copy-start(f32[3,704]{1,0:T(4,128)} %param.26) | copy-start | bytes 25348
  207.7 77.8 %copy-start.6 = (f32[3,704]{1,0:T(4,128)S(1)}, f32[3,704]{1,0:T(4,128)}, u32[]{:S(2)}) copy-start(f32[3,704]{1,0:T(4,128)} %param.25) | copy-start | bytes 25348
  280.9 4.6 %collective-permute-start = (bf16[1,1408]{1,0:T(2,128)(2,1)S(1)}, bf16[1,1408]{1,0:T(2,128)(2,1)S(1)}, u32[]{:S(2)}, u32[]{:S(2)}) collective-permute-start(bf16[1,1408]{1,0:T(2,128)(2,1)S(1)} %get-tuple-element.10), channel_id=1, source_target_pairs={{0,8},{8,16},{16,24},{24,32},{32,40},{40,48},{48,56},{56,64},{64,7... | collective-permute-start | bytes 8456 | tf_op jit(solution)/shard_map/ppermute | solution.py:38
  284.1 4.4 %collective-permute-start.1 = (bf16[1,1408]{1,0:T(2,128)(2,1)S(1)}, bf16[1,1408]{1,0:T(2,128)(2,1)S(1)}, u32[]{:S(2)}, u32[]{:S(2)}) collective-permute-start(bf16[1,1408]{1,0:T(2,128)(2,1)S(1)} %get-tuple-element.11), channel_id=1, source_target_pairs={{8,0},{16,8},{24,16},{32,24},{40,32},{48,40},{56,48},{64,56},{72,6... | collective-permute-start | bytes 8456 | tf_op jit(solution)/shard_map/ppermute | solution.py:41
  295.3 43.4 %copy-start.1 = (bf16[128,2048]{1,0:T(8,128)(2,1)S(1)}, bf16[128,2048]{1,0:T(8,128)(2,1)}, u32[]{:S(2)}) copy-start(bf16[128,2048]{1,0:T(8,128)(2,1)} %param.20) | copy-start | bytes 1572868
Sparse Core Ops, SparseCore 0:
  13.5 95.9 all-gather.3
  111.3 118.8 all-gather.7
  232.0 40.3 all-gather.5
where the time goes:
time: 346 us; the launch traced here: 345 us
  waiting for transfers between devices  161 us (47%)
  blocking collectives  87.7 us (25%)
  matrix products  48.5 us (14%)
  other arithmetic  28.9 us (8%)
  between operations  13.4 us (4%)
  starting transfers between devices  4.63 us (1%)
    all_gather x2, waiting for transfers between devices, sent_together(): lax.all_gather(both, axis, axis=dim, tiled=True)  116 us
    all_to_all x2, blocking collectives, summed_on_arrival(): lax.all_to_all(tiles, axis, split_axis=0, concat_axis=0, tiled=True)  87.7 us
    all_gather x1, waiting for transfers between devices, body(): lax.all_gather(normed, 'tp', axis=0, tiled=True)  42.3 us
    dot_general x1, matrix products, body(): jnp.dot(block_rows, out_weight, preferred_element_type=jnp.float32)  18.7 us
    dot_general x1, matrix products, body(): lax.dot_general(query_rows, key_piece, (((1,), (1,)), ((), ())), preferre...  16.3 us
    reduce_sum x1, other arithmetic, body(): denom = jnp.sum(weights, axis=1, keepdims=True)  15.4 us
    dot_general x1, matrix products, body(): jnp.dot(lax.all_gather(normed, 'tp', axis=0, tiled=True), paired, preferr...  8.42 us
  transfers between devices with their start and end apart: 5, of which 4 were waited for; matrix products, arithmetic and copies ran while one was open for 16% of the time, Pallas kernels for 0%

commit v1 on v0

--- a/solution.py
+++ b/solution.py
@@ -8,6 +8,28 @@
 GRID_W = 64
 EPSILON = 1e-06
 THETA = 10000.0
+
+
+def laid_out(tiles, dim):
+    shape = list(tiles.shape[1:])
+    shape[dim] *= tiles.shape[0]
+    return jnp.moveaxis(tiles, 0, dim).reshape(shape)
+
+
+def collect(shard, axis, dim):
+    peers = lax.axis_size(axis)
+    pairs = [(i, (i + 1) % peers) for i in range(peers)]
+    back = [(b, a) for a, b in pairs]
+    lower, upper = ([], [])
+    for lap in range(peers - 1):
+        if lap % 2 == 0:
+            lower.append(lax.ppermute(lower[-1] if lower else shard, axis, pairs))
+        else:
+            upper.append(lax.ppermute(upper[-1] if upper else shard, axis, back))
+    blocks = jnp.stack([*lower[::-1], shard, *upper])
+    shift = lax.axis_index(axis) - len(lower)
+    blocks = blocks[(jnp.arange(peers) - shift) % peers]
+    return laid_out(blocks, dim)
 
 
 def sent_together(arrays, axis, dim, along):
@@ -128,9 +150,9 @@
     stream = (residual.astype(jnp.float32) + rms_rows(mix, mix_gain)).astype(jnp.bfloat16)
     normed = rms_rows(stream, ffn_gain).astype(jnp.bfloat16)
     paired = jnp.concatenate([gate_rows, value_rows], axis=1)
-    upward = jnp.dot(
-        lax.all_gather(normed, "tp", axis=0, tiled=True), paired, preferred_element_type=jnp.float32
-    ).astype(jnp.bfloat16)
+    upward = jnp.dot(collect(normed, "tp", 0), paired, preferred_element_type=jnp.float32).astype(
+        jnp.bfloat16
+    )
     padded = with_halo(upward, (("sp", 0),), 1).astype(jnp.float32)
     taps = jnp.concatenate([conv_gate, conv_value], axis=1)
     mixed = taps[0] * padded[:-2] + taps[1] * padded[1:-1] + taps[2] * padded[2:]

time: 346 us -> 324 us (0.936)
  waiting for transfers between devices: 161 us -> 110 us
  starting transfers between devices: 4.63 us -> 17.6 us
  local copies, waits for them, and re-layouts: 1.02 us -> 10.1 us
  blocking collectives: 87.7 us -> 93.9 us
    all_gather x1 -> x0, waiting for transfers between devices: 42.3 us -> none  [body(): lax.all_gather(normed, 'tp', axis=0, tiled=True)]
    all_gather x2, waiting for transfers between devices: 116 us -> 93.3 us  [sent_together(): lax.all_gather(both, axis, axis=dim, tiled=True)]
    ppermute x0 -> x7, waiting for transfers between devices: none -> 14 us  [the longest x4 13 us: collect(): lower.append(lax.ppermute(lower[-1] if lower else shard, axis, pairs))]
    ppermute x0 -> x7, starting transfers between devices: none -> 13.9 us  [the longest x4 9.02 us: collect(): lower.append(lax.ppermute(lower[-1] if lower else shard, axis, pairs))]
    all_to_all x2, blocking collectives: 87.7 us -> 93.9 us  [summed_on_arrival(): lax.all_to_all(tiles, axis, split_axis=0, concat_axis=0, tiled=True)]
    unnamed x22 -> x30, local copies, waits for them, and re-layouts: 0.05 us -> 5.02 us
    gather x0 -> x1, local copies, waits for them, and re-layouts: none -> 4.29 us  [collect(): blocks = blocks[(jnp.arange(peers) - shift) % peers]]
  transfers between devices with their start and end apart: 5 -> 11, of which waited for: 4 -> 8; matrix products, arithmetic and copies ran while one was open for 16% -> 20% of each run, Pallas kernels for 0% -> 0%
where the time goes in v1:
time: 324 us; the launch traced here: 323 us
  waiting for transfers between devices  110 us (34%)
  blocking collectives  93.9 us (29%)
  matrix products  48.5 us (15%)
  other arithmetic  29.1 us (9%)
  starting transfers between devices  17.6 us (5%)
  between operations  13.7 us (4%)
  local copies, waits for them, and re-layouts  10.1 us (3%)
    all_to_all x2, blocking collectives, summed_on_arrival(): lax.all_to_all(tiles, axis, split_axis=0, concat_axis=0, tiled=True)  93.9 us
    all_gather x2, waiting for transfers between devices, sent_together(): lax.all_gather(both, axis, axis=dim, tiled=True)  93.3 us
    dot_general x1, matrix products, body(): jnp.dot(block_rows, out_weight, preferred_element_type=jnp.float32)  18.7 us
    dot_general x1, matrix products, body(): lax.dot_general(query_rows, key_piece, (((1,), (1,)), ((), ())), preferre...  16.3 us
    reduce_sum x1, other arithmetic, body(): denom = jnp.sum(weights, axis=1, keepdims=True)  15.4 us
    ppermute x4, waiting for transfers between devices, collect(): lower.append(lax.ppermute(lower[-1] if lower else shard, axis, pairs))  13 us
    ppermute x4, starting transfers between devices, collect(): lower.append(lax.ppermute(lower[-1] if lower else shard, axis, pairs))  9.02 us
    dot_general x1, matrix products, body(): jnp.dot(collect(normed, 'tp', 0), paired, preferred_element_type=jnp.floa...  8.44 us
  transfers between devices with their start and end apart: 11, of which 8 were waited for; matrix products, arithmetic and copies ran while one was open for 20% of the time, Pallas kernels for 0%

profile of v1, /device:TPU:33, one launch (start us, length us, event | category | flops | bytes accessed | tf_op | source)
XLA Modules:
  0.0 323.3 jit_solution(18131975368113705969)
XLA Ops:
  6.7 1.2 fusion.55
  7.9 1.1 fusion.56
  9.7 2.0 fusion.60
  11.7 0.8 pad_maximum_fusion.2
  12.7 1.9 pad_maximum_fusion
  15.4 93.3 %all-gather.3.cloned.1.call-done = bf16[12288,256]{1,0:T(8,128)(2,1)} async-done(((bf16[768,256]{1,0:T(8,128)(2,1)}), bf16[12288,256]{1,0:T(8,128)(2,1)}) %all-gather.3.cloned.1.call-update) | async-done | bytes 6291472 | tf_op jit(solution)/shard_map/all_gather | solution.py:37
  108.7 16.3 %fusion.89 = (f32[768]{0:T(1024)S(1)}, f32[768,12288]{1,0:T(8,128)}) fusion(bf16[12288,256]{1,0:T(8,128)(2,1)} %all-gather.3.cloned.1.call-done, bf16[768,128]{1,0:T(8,128)(2,1)S(1)} %copy-done.2, f32[768,32]{1,0:T(8,128)S(1)} %get-tuple-element.13, f32[768,32]{1,0:T(8,128)S(1)} %get-tuple-element.14, f32[768,32]{1,0:T(8,128)S(1)} %get-tuple-element.15, ...), kind=kOutput, calls=%fused_computation.133 | convolution fusion | flops 2426731776 | bytes 41687552 | tf_op jit(solution)/shard_map/dot_general | solution.py:134
  125.0 15.4 %fusion = f32[768]{0:T(1024)S(1)} fusion(f32[768,12288]{1,0:T(8,128)} %get-tuple-element.23, f32[768]{0:T(1024)S(1)} %broadcast_maximum_fusion), kind=kLoop, calls=%fused_computation.2 | loop fusion | flops 18873600 | bytes 37754880 | tf_op jit(solution)/shard_map/reduce_sum | solution.py:139
  140.4 18.7 %convolution_convert_fusion.1 = bf16[768,2048]{1,0:T(8,128)(2,1)} fusion(bf16[128,2048]{1,0:T(8,128)(2,1)S(1)} %copy-done, bf16[12288,256]{1,0:T(8,128)(2,1)} %all-gather.3.cloned.1.call-done, f32[768,12288]{1,0:T(8,128)} %get-tuple-element.23, f32[768]{0:T(1024)S(1)} %broadcast_maximum_fusion, f32[768]{0:T(1024)S(1)} %fusion), kind=kOutput, calls=%fused_computation.17 | convolution fusion | flops 2839216128 | bytes 44570624 | tf_op jit(solution)/shard_map/dot_general | solution.py:146
  159.1 45.6 %all_to_all.10 = bf16[8,96,2048]{2,1,0:T(8,128)(2,1)S(1)} all-to-all(bf16[8,96,2048]{2,1,0:T(8,128)(2,1)} %bitcast.33), channel_id=1, replica_groups=mesh['grp'=2,'sp'=16,'tp'=8] {'tp'}, dimensions={0} | all-to-all | bytes 6291456 | tf_op jit(solution)/shard_map/all_to_all | solution.py:51
  206.2 1.6 collective-permute-start
  207.7 4.7 %collective-permute-done = bf16[96,2048]{1,0:T(8,128)(2,1)S(1)} collective-permute-done((bf16[96,2048]{1,0:T(8,128)(2,1)S(1)}, bf16[96,2048]{1,0:T(8,128)(2,1)S(1)}, u32[]{:S(2)}, u32[]{:S(2)}) %collective-permute-start) | collective-permute-done | bytes 393248 | tf_op jit(solution)/shard_map/ppermute | solution.py:26
  212.5 2.5 collective-permute-start.1
  215.6 4.1 %collective-permute-done.1 = bf16[96,2048]{1,0:T(8,128)(2,1)S(1)} collective-permute-done((bf16[96,2048]{1,0:T(8,128)(2,1)S(1)}, bf16[96,2048]{1,0:T(8,128)(2,1)S(1)}, u32[]{:S(2)}, u32[]{:S(2)}) %collective-permute-start.1) | collective-permute-done | bytes 393248 | tf_op jit(solution)/shard_map/ppermute | solution.py:26
  219.7 2.5 collective-permute-start.2
  222.4 1.6 collective-permute-start.5
  224.0 2.8 collective-permute-done.2
  226.9 2.5 collective-permute-start.3
  230.0 2.6 collective-permute-start.6
  232.7 1.4 collective-permute-done.3
  237.2 0.9 bitcast_dynamic-update-slice_fusion.3
  238.1 0.8 bitcast_dynamic-update-slice_fusion.2
  238.9 0.8 bitcast_dynamic-update-slice_fusion.1
  240.5 4.3 %gather_fusion = bf16[8,96,2048]{2,1,0:T(8,128)(2,1)} fusion(bf16[8,96,2048]{2,1,0:T(8,128)(2,1)} %bitcast_dynamic-update-slice_fusion, s32[1024]{0:T(1024)S(1)} %pad_clamp_fusion), kind=kCustom, calls=%fused_computation | custom fusion | bytes 6291488 | tf_op jit(solution)/shard_map/gather | solution.py:31
  244.8 8.4 %fusion.9 = bf16[768,1408]{1,0:T(8,128)(2,1)S(1)} fusion(bf16[768,2048]{1,0:T(8,128)(2,1)} %bitcast.34, bf16[2048,2112]{0,1:T(8,128)(2,1)} %all-gather.5.cloned.1.call-done), kind=kOutput, calls=%fused_computation.18 | convolution fusion | flops 4430266368 | bytes 11075584 | tf_op jit(solution)/shard_map/dot_general | solution.py:153
  253.2 2.3 collective-permute-start.7
  255.5 1.3 collective-permute-start.8
  257.0 2.9 collective-permute-done.8
  260.4 1.3 fusion.7
  261.6 5.1 %convolution_convert_fusion = bf16[768,2048]{1,0:T(8,128)(2,1)S(1)} fusion(bf16[2048,2112]{0,1:T(8,128)(2,1)} %all-gather.5.cloned.1.call-done, f32[768,1408]{1,0:T(8,128)S(1)} %fusion.7), kind=kOutput, calls=%fused_computation.16 | convolution fusion | flops 2221572096 | bytes 10747904 | tf_op jit(solution)/shard_map/dot_general | solution.py:165
  266.8 48.3 %all_to_all.11 = bf16[8,96,2048]{2,1,0:T(8,128)(2,1)S(1)} all-to-all(bf16[8,96,2048]{2,1,0:T(8,128)(2,1)S(1)} %bitcast.35), channel_id=1, replica_groups=mesh['grp'=2,'sp'=16,'tp'=8] {'tp'}, dimensions={0} | all-to-all | bytes 6291456 | tf_op jit(solution)/shard_map/all_to_all | solution.py:51
  315.6 0.8 fusion.47
  (62 shorter events, 9.8 us)
Async XLA Ops:
  6.5 133.8 %copy-start = (bf16[128,2048]{1,0:T(8,128)(2,1)S(1)}, bf16[128,2048]{1,0:T(8,128)(2,1)}, u32[]{:S(2)}) copy-start(bf16[128,2048]{1,0:T(8,128)(2,1)} %param.20) | copy-start | bytes 1572868
  6.6 3.2 copy-start.3
  6.6 3.2 copy-start.11
  6.6 2.8 copy-start.5
  6.6 102.1 %all-gather.3.cloned.1.call-start = ((), (), s32[]{:S(2)}) async-start(), calls=%async_computation.2 | async-start | bytes 6684672 | tf_op jit(solution)/shard_map/all_gather | solution.py:37
  9.4 5.2 %copy-start.2 = (bf16[768,128]{1,0:T(8,128)(2,1)S(1)}, bf16[768,128]{1,0:T(8,128)(2,1)}, u32[]{:S(2)}) copy-start(bf16[768,128]{1,0:T(8,128)(2,1)} %param.14) | copy-start | bytes 589828
  9.4 5.4 %copy-start.10 = (f32[128]{0:T(128)S(1)}, f32[128]{0:T(128)}, u32[]{:S(2)}) copy-start(f32[128]{0:T(128)} %param.17) | copy-start | bytes 1540
  12.6 232.2 %all-gather.5.cloned.1.call-start = ((), (), s32[]{:S(2)}) async-start(), calls=%async_computation.3 | async-start | bytes 9191424 | tf_op jit(solution)/shard_map/all_gather | solution.py:37
  204.6 1.0 copy-start.4
  204.6 1.0 copy-start.9
  204.6 1.3 copy-start.6
  206.2 6.3 %collective-permute-start = (bf16[96,2048]{1,0:T(8,128)(2,1)S(1)}, bf16[96,2048]{1,0:T(8,128)(2,1)S(1)}, u32[]{:S(2)}, u32[]{:S(2)}) collective-permute-start(bf16[96,2048]{1,0:T(8,128)(2,1)S(1)} %fusion.46), channel_id=1, source_target_pairs={{0,1},{1,2},{2,3},{3,4},{4,5},{5,6},{6,7},{7,0},{8,9},{9,10},{10,1... | collective-permute-start | bytes 1179656 | tf_op jit(solution)/shard_map/ppermute | solution.py:26
  212.5 7.2 %collective-permute-start.1 = (bf16[96,2048]{1,0:T(8,128)(2,1)S(1)}, bf16[96,2048]{1,0:T(8,128)(2,1)S(1)}, u32[]{:S(2)}, u32[]{:S(2)}) collective-permute-start(bf16[96,2048]{1,0:T(8,128)(2,1)S(1)} %collective-permute-done), channel_id=1, source_target_pairs={{0,1},{1,2},{2,3},{3,4},{4,5},{5,6},{6,7},{7,0},{8,9},{9,10},{10,1... | collective-permute-start | bytes 1179656 | tf_op jit(solution)/shard_map/ppermute | solution.py:26
  214.9 7.5 %collective-permute-start.4 = (bf16[96,2048]{1,0:T(8,128)(2,1)S(1)}, bf16[96,2048]{1,0:T(8,128)(2,1)S(1)}, u32[]{:S(2)}, u32[]{:S(2)}) collective-permute-start(bf16[96,2048]{1,0:T(8,128)(2,1)S(1)} %fusion.46), channel_id=1, source_target_pairs={{1,0},{2,1},{3,2},{4,3},{5,4},{6,5},{7,6},{0,7},{9,8},{10,9},{11,1... | collective-permute-start | bytes 1179656 | tf_op jit(solution)/shard_map/ppermute | solution.py:28
  219.7 7.2 %collective-permute-start.2 = (bf16[96,2048]{1,0:T(8,128)(2,1)S(1)}, bf16[96,2048]{1,0:T(8,128)(2,1)S(1)}, u32[]{:S(2)}, u32[]{:S(2)}) collective-permute-start(bf16[96,2048]{1,0:T(8,128)(2,1)S(1)} %collective-permute-done.1), channel_id=1, source_target_pairs={{0,1},{1,2},{2,3},{3,4},{4,5},{5,6},{6,7},{7,0},{8,9},{9,10},{10,1... | collective-permute-start | bytes 1179656 | tf_op jit(solution)/shard_map/ppermute | solution.py:26
  222.4 7.6 %collective-permute-start.5 = (bf16[96,2048]{1,0:T(8,128)(2,1)S(1)}, bf16[96,2048]{1,0:T(8,128)(2,1)S(1)}, u32[]{:S(2)}, u32[]{:S(2)}) collective-permute-start(bf16[96,2048]{1,0:T(8,128)(2,1)S(1)} %collective-permute-done.4), channel_id=1, source_target_pairs={{1,0},{2,1},{3,2},{4,3},{5,4},{6,5},{7,6},{0,7},{9,8},{10,9},{11,1... | collective-permute-start | bytes 1179656 | tf_op jit(solution)/shard_map/ppermute | solution.py:28
  226.9 7.2 %collective-permute-start.3 = (bf16[96,2048]{1,0:T(8,128)(2,1)S(1)}, bf16[96,2048]{1,0:T(8,128)(2,1)S(1)}, u32[]{:S(2)}, u32[]{:S(2)}) collective-permute-start(bf16[96,2048]{1,0:T(8,128)(2,1)S(1)} %collective-permute-done.2), channel_id=1, source_target_pairs={{0,1},{1,2},{2,3},{3,4},{4,5},{5,6},{6,7},{7,0},{8,9},{9,10},{10,1... | collective-permute-start | bytes 1179656 | tf_op jit(solution)/shard_map/ppermute | solution.py:26
  230.0 9.6 %collective-permute-start.6 = (bf16[96,2048]{1,0:T(8,128)(2,1)S(1)}, bf16[96,2048]{1,0:T(8,128)(2,1)S(1)}, u32[]{:S(2)}, u32[]{:S(2)}) collective-permute-start(bf16[96,2048]{1,0:T(8,128)(2,1)S(1)} %collective-permute-done.5), channel_id=1, source_target_pairs={{1,0},{2,1},{3,2},{4,3},{5,4},{6,5},{7,6},{0,7},{9,8},{10,9},{11,1... | collective-permute-start | bytes 1179656 | tf_op jit(solution)/shard_map/ppermute | solution.py:28
  244.8 12.1 %copy-start.7 = (f32[3,704]{1,0:T(4,128)S(1)}, f32[3,704]{1,0:T(4,128)}, u32[]{:S(2)}) copy-start(f32[3,704]{1,0:T(4,128)} %param.26) | copy-start | bytes 25348
  244.8 12.1 %copy-start.8 = (f32[3,704]{1,0:T(4,128)S(1)}, f32[3,704]{1,0:T(4,128)}, u32[]{:S(2)}) copy-start(f32[3,704]{1,0:T(4,128)} %param.25) | copy-start | bytes 25348
  253.2 3.7 %collective-permute-start.7 = (bf16[1,1408]{1,0:T(2,128)(2,1)S(1)}, bf16[1,1408]{1,0:T(2,128)(2,1)S(1)}, u32[]{:S(2)}, u32[]{:S(2)}) collective-permute-start(bf16[1,1408]{1,0:T(2,128)(2,1)S(1)} %get-tuple-element.10), channel_id=1, source_target_pairs={{0,8},{8,16},{16,24},{24,32},{32,40},{40,48},{48,56},{56,64},{64,7... | collective-permute-start | bytes 8456 | tf_op jit(solution)/shard_map/ppermute | solution.py:60
  255.5 4.4 %collective-permute-start.8 = (bf16[1,1408]{1,0:T(2,128)(2,1)S(1)}, bf16[1,1408]{1,0:T(2,128)(2,1)S(1)}, u32[]{:S(2)}, u32[]{:S(2)}) collective-permute-start(bf16[1,1408]{1,0:T(2,128)(2,1)S(1)} %get-tuple-element.11), channel_id=1, source_target_pairs={{8,0},{16,8},{24,16},{32,24},{40,32},{48,40},{56,48},{64,56},{72,6... | collective-permute-start | bytes 8456 | tf_op jit(solution)/shard_map/ppermute | solution.py:63
  266.8 49.7 %copy-start.1 = (bf16[128,2048]{1,0:T(8,128)(2,1)S(1)}, bf16[128,2048]{1,0:T(8,128)(2,1)}, u32[]{:S(2)}) copy-start(bf16[128,2048]{1,0:T(8,128)(2,1)} %param.20) | copy-start | bytes 1572868
Sparse Core Ops, SparseCore 0:
  12.7 95.9 all-gather.2
  110.4 118.9 all-gather.4
